TPU v7x, 32 devices: a whole 2x2x4 slice. The times are simulated.
32 devices in a mesh: ep: 8 (over z, x), tp: 4 (over y, core).
Axes of the slice: x: 2, y: 2, z: 4, core: 2. Of those that a mesh axis runs over, the one named last changes fastest.
Arguments:
- query_logits: bfloat16 [2048, 2048], P('ep', 'tp'), may hold values from -6 to 6
- forget_gate_logits: bfloat16 [2048, 2048], P('ep', 'tp'), may hold values from -3.75 to 3.75
- written_values: bfloat16 [2048, 2048], P('ep', 'tp'), may hold values from -6 to 6
- output_gate_logits: bfloat16 [2048, 2048], P('ep', 'tp'), may hold values from -6 to 6
- gap: float32 [2048], P('tp'), may hold values from 4.8828125e-05 to 0.06
- extra_log_forget: float32 [2048, 2048], P('ep', 'tp'), may hold values from -0.7 to 0
- head_norm_scale: float32 [2048], P('tp'), may hold values from 0.1 to 1.9
- mixer_output_matrix: bfloat16 [2048, 2048], P('tp'), may hold values from -0.125 to 0.125
- expert_input_tokens: bfloat16 [2048, 2048], P('ep'), may hold values from -12 to 12
- expert_norm_scale: float32 [2048], replicated, may hold values from 0.1 to 1.9
- routes: int32 [2048, 2], P('ep'), may hold values from 0 to 7, all different within a row; in each aligned block of 256 rows (0 to 255, 256 to 511, ...) at most 96 rows name the same one
- router_scores_chosen: float32 [2048, 2], P('ep'), may hold values from -6 to 6
- expert_gate_matrix: bfloat16 [8, 2048, 4096], P('ep', None, 'tp'), may hold values from -0.125 to 0.125
- expert_up_matrix: bfloat16 [8, 2048, 4096], P('ep', None, 'tp'), may hold values from -0.125 to 0.125
- expert_down_matrix: bfloat16 [8, 2048, 4096], P('ep', None, 'tp'), may hold values from -0.09375 to 0.09375
Outputs:
- mixer_output_rows: bfloat16 [2048, 2048], P(('ep', 'tp'))
- expert_out: bfloat16 [2048, 2048], P('ep', 'tp')
Inputs may be any that keep to these rules, and one draw needn't show every extreme that they name: `routes`: each row names two different experts. Among the rows of one device no expert is named more than 96 times, and 96 is reached in some blocks.
All inputs are finite; a program needn't handle non-finite values.
Results may differ from a plain program's by a relative error of at most 0.019.
Values may be sent and summed in bfloat16 or wider, within the bound.
A program may use at most 64 MiB of HBM per device.

v0:
```python
import functools

import jax
import jax.numpy as jnp
from jax import lax
from jax.experimental import pallas as pl
from jax.experimental.pallas import tpu as pltpu
from jax.sharding import PartitionSpec as P

HEAD_DIM = 128
CHUNK = 64
MESH = pl.DeviceIdType.MESH
F32 = jnp.float32
BF16 = jnp.bfloat16


def flip(i, k):
    b = 1
    while b <= k:
        if k & b:
            i = i + b - 2 * b * lax.rem(lax.div(i, b), 2)
        b *= 2
    return i


def kernel(
    E, T, cap, pieces,
    q_ref, f_ref, v_ref, o_ref, gap_ref, extra_ref, hscale_ref,
    mixw_hbm, tok_ref, escale_ref, routes_ref, scores_ref,
    gate_hbm, up_hbm, down_hbm,
    mix_out, exp_out,
    gate, up, down, mixw,
    ncols, dmat, wmat, outgoing, feats, hidden, part, precv, xsend, xrecv, fin, ret,
    qs, ks, run, qg, rec, ist, idec, est, edec, ksend, krecv,
    mhid, mpart, mprecv, mxsend, mxrecv,
    wsem, send_sem, recv_sem,
):
    me = lax.axis_index("ep")
    t = lax.axis_index("tp")
    G = T // 2
    g, c = lax.div(t, 2), lax.rem(t, 2)
    oc = 1 - c
    tokens, width = q_ref.shape
    heads = width // HEAD_DIM
    S = E * cap
    Dl = ncols.shape[1]
    FFl = hidden.shape[1]

    loads = [
        pltpu.make_async_copy(src, dst, wsem.at[i])
        for i, (src, dst) in enumerate(
            ((gate_hbm, gate), (up_hbm, up), (down_hbm, down), (mixw_hbm, mixw))
        )
    ]
    for load in loads:
        load.start()

    barrier = pltpu.get_barrier_semaphore()
    for k in range(1, E):
        pl.semaphore_signal(barrier, inc=1, device_id=(flip(me, k), t), device_id_type=MESH)
    pl.semaphore_signal(barrier, inc=1, device_id=(me, 2 * g + oc), device_id_type=MESH)
    for j in range(1, G):
        pl.semaphore_signal(
            barrier, inc=1, device_id=(me, 2 * flip(g, j) + c), device_id_type=MESH
        )

    used = [0]

    def remote(src, dst, device):
        slot = used[0]
        used[0] += 1
        return pltpu.make_async_remote_copy(
            src_ref=src, dst_ref=dst, send_sem=send_sem.at[slot], recv_sem=recv_sem.at[slot],
            device_id=device, device_id_type=MESH,
        )

    sent = []

    x = tok_ref[...].astype(F32)
    mean = jnp.mean(x, axis=-1, keepdims=True)
    centred = x - mean
    inv = lax.rsqrt(jnp.mean(centred * centred, axis=-1, keepdims=True) + 1e-05)
    cols = pl.ds(pl.multiple_of(t * Dl, 128), Dl)
    ncols[...] = ((tok_ref[:, cols].astype(F32) - mean) * inv * escale_ref[:, cols]).astype(BF16)

    ntok = tok_ref.shape[0]
    ek = lax.broadcasted_iota(jnp.int32, (E, ntok), 0) ^ me
    first, second = routes_ref[0:1, :] == ek, routes_ref[1:2, :] == ek
    named = jnp.where(first | second, 1.0, 0.0)
    earlier = jnp.where(
        lax.broadcasted_iota(jnp.int32, (ntok, ntok), 0)
        < lax.broadcasted_iota(jnp.int32, (ntok, ntok), 1), 1.0, 0.0
    ).astype(BF16)
    position = jnp.dot(named.astype(BF16), earlier, preferred_element_type=F32)
    place = jnp.where(first | second, position, -1.0).astype(jnp.int32)
    w0 = jax.nn.sigmoid(scores_ref[0:1, :] - scores_ref[1:2, :])
    weight = jnp.where(first, w0, jnp.where(second, 1.0 - w0, 0.0))
    rows = lax.broadcasted_iota(jnp.int32, (cap, ntok), 0)
    for k in range(E):
        hit = rows == place[k:k + 1, :]
        dmat[k * cap:(k + 1) * cap, :] = jnp.where(hit, 1.0, 0.0).astype(BF16)
        wmat[k * cap:(k + 1) * cap, :] = jnp.where(hit, weight[k:k + 1, :], 0.0).astype(BF16)
    outgoing[...] = jnp.dot(dmat[...], ncols[...], preferred_element_type=F32).astype(BF16)
    feats[t, 0:cap, :] = outgoing[0:cap, :]

    pl.semaphore_wait(barrier, E - 1 + 1 + G - 1)

    dispatch = {}
    for k in range(1, E):
        block = pl.ds(k * cap, cap)
        dispatch[k] = remote(outgoing.at[block], feats.at[t, block], (flip(me, k), t))
        dispatch[k].start()
        sent.append(dispatch[k])

    closing = gap_ref[...] * jax.nn.sigmoid(-f_ref[...].astype(F32))
    ks[...] = closing
    logd = jnp.log1p(-closing) + extra_ref[...]
    qs[...] = jax.nn.silu(q_ref[...].astype(F32))
    r_i = lax.broadcasted_iota(jnp.int32, (CHUNK, CHUNK), 0)
    c_i = lax.broadcasted_iota(jnp.int32, (CHUNK, CHUNK), 1)
    causal = r_i >= c_i
    tri = jnp.where(causal, 1.0, 0.0).astype(F32)
    nchunks = tokens // CHUNK
    for n in range(nchunks):
        run[n * CHUNK:(n + 1) * CHUNK, :] = jnp.dot(
            tri, logd[n * CHUNK:(n + 1) * CHUNK, :], precision=lax.Precision.HIGHEST,
            preferred_element_type=F32,
        )

    def head_local(h, _):
        lanes = pl.ds(pl.multiple_of(h * HEAD_DIM, HEAD_DIM), HEAD_DIM)
        state = jnp.zeros((HEAD_DIM, HEAD_DIM), F32)
        before = jnp.zeros((1, HEAD_DIM), F32)
        for n in range(nchunks):
            rs = slice(n * CHUNK, (n + 1) * CHUNK)
            r = run[rs, lanes]
            total = r[CHUNK - 1:CHUNK, :]
            qd = qs[rs, lanes] * jnp.exp(r)
            key = ks[rs, lanes]
            kd = (key * jnp.exp(-r)).astype(BF16)
            kst = (key * jnp.exp(total - r)).astype(BF16)
            val = v_ref[rs, lanes]
            qd_b = qd.astype(BF16)
            scores = lax.dot_general(
                qd_b, kd, (((1,), (1,)), ((), ())), preferred_element_type=F32
            )
            scores = jnp.where(causal, scores, 0.0).astype(BF16)
            out = jnp.dot(scores, val, preferred_element_type=F32)
            if n:
                out += lax.dot_general(
                    qd_b, state.astype(BF16), (((1,), (1,)), ((), ())),
                    preferred_element_type=F32,
                )
            rec[rs, lanes] = out
            qg[rs, lanes] = (qd * jnp.exp(before)).astype(BF16)
            state = state * jnp.exp(total) + lax.dot_general(
                val, kst, (((0,), (0,)), ((), ())), preferred_element_type=F32
            )
            before = before + total
        ist[h] = state
        idec[h] = jnp.broadcast_to(jnp.exp(before), (16, HEAD_DIM))
        est[h] = jnp.zeros((HEAD_DIM, HEAD_DIM), F32)
        edec[h] = jnp.ones((16, HEAD_DIM), F32)
        return 0

    lax.fori_loop(0, heads, head_local, 0)

    hops = []
    dist = 1
    while dist < E:
        hops.append(dist)
        dist *= 2
    hop_copy = [
        remote(ksend.at[r], krecv.at[r], (lax.rem(me + d, E), t)) for r, d in enumerate(hops)
    ]

    def hop_send(r):
        @pl.when(me + hops[r] < E)
        def _():
            ksend[r, :, 0:HEAD_DIM, :] = ist[...].astype(BF16)
            ksend[r, :, HEAD_DIM:HEAD_DIM + 16, :] = idec[...].astype(BF16)
            hop_copy[r].start()

    def hop_recv(r):
        @pl.when(me >= hops[r])
        def _():
            hop_copy[r].wait_recv()
            s = krecv[r, :, 0:HEAD_DIM, :].astype(F32)
            d = krecv[r, :, HEAD_DIM:HEAD_DIM + 16, :].astype(F32)
            est[...] = edec[:, 0:1, :] * s + est[...]
            edec[...] = edec[...] * d
            if r + 1 < len(hops):
                ist[...] = idec[:, 0:1, :] * s + ist[...]
                idec[...] = idec[...] * d

    hop_send(0)

    ag_partner, ag_cross, rs_partner, rs_cross, back = {}, {}, {}, {}, {}

    def piece_rows(p):
        a, n = pieces[p]
        return pl.ds(a * cap, n * cap)

    def gather_start(p):
        a, n = pieces[p]
        for k in range(max(a, 1), a + n):
            dispatch[k].wait_recv()
        rr = piece_rows(p)
        for j in range(1, G):
            ag_cross[p, j] = remote(feats.at[t, rr], feats.at[t, rr], (me, 2 * flip(g, j) + c))
            ag_cross[p, j].start()
            sent.append(ag_cross[p, j])
        for j in range(G):
            idx = 2 * flip(g, j) + c
            ag_partner[p, j] = (
                used[0], remote(feats.at[idx, rr], feats.at[idx, rr], (me, 2 * g + oc))
            )
        ag_partner[p, 0][1].start()
        sent.append(ag_partner[p, 0][1])

    def gather_relay(p):
        rr = piece_rows(p)
        for j in range(1, G):
            ag_cross[p, j].wait_recv()
            ag_partner[p, j][1].start()
            sent.append(ag_partner[p, j][1])

    def gather_end(p):
        for j in range(G):
            ag_partner[p, j][1].wait_recv()

    tile = min(256, FFl)

    def experts(p):
        a, n = pieces[p]
        rs = slice(a * cap, (a + n) * cap)

        def one(i, _):
            cc = pl.ds(pl.multiple_of(i * tile, tile), tile)
            ga = jnp.zeros((n * cap, tile), F32)
            ua = jnp.zeros((n * cap, tile), F32)
            for d in range(T):
                xs = feats[d, rs, :]
                ga += jnp.dot(xs, gate[d * Dl:(d + 1) * Dl, cc], preferred_element_type=F32)
                ua += jnp.dot(xs, up[d * Dl:(d + 1) * Dl, cc], preferred_element_type=F32)
            hidden[rs, cc] = (jax.nn.silu(ga) * ua).astype(BF16)
            return 0

        lax.fori_loop(0, FFl // tile, one, 0)

        def down_group(cls, gg):
            ff = pl.ds(pl.multiple_of((2 * gg + cls) * Dl, 128), Dl)
            part[cls, gg, rs, :] = lax.dot_general(
                hidden[rs, :], down[ff, :], (((1,), (1,)), ((), ())),
                preferred_element_type=F32,
            ).astype(BF16)

        def theirs(gg, _):
            down_group(oc, gg)
            return 0

        def ours(gg, _):
            down_group(c, gg)
            return 0

        lax.fori_loop(0, G, theirs, 0)
        rr = piece_rows(p)
        rs_partner[p] = remote(part.at[oc, :, rr], precv.at[:, rr], (me, 2 * g + oc))
        rs_partner[p].start()
        sent.append(rs_partner[p])
        lax.fori_loop(0, G, ours, 0)

    def scatter_cross(p):
        a, n = pieces[p]
        rs = slice(a * cap, (a + n) * cap)
        rr = piece_rows(p)
        rs_partner[p].wait_recv()
        for j in range(1, G):
            gj = flip(g, j)
            xsend[j - 1, rs, :] = (
                part[c, gj, rs, :].astype(F32) + precv[gj, rs, :].astype(F32)
            ).astype(BF16)
            rs_cross[p, j] = remote(
                xsend.at[j - 1, rr], xrecv.at[j - 1, rr], (me, 2 * gj + c)
            )
            rs_cross[p, j].start()
            sent.append(rs_cross[p, j])

    def give_back(p):
        a, n = pieces[p]
        rs = slice(a * cap, (a + n) * cap)
        total = part[c, g, rs, :].astype(F32) + precv[g, rs, :].astype(F32)
        for j in range(1, G):
            rs_cross[p, j].wait_recv()
            total += xrecv[j - 1, rs, :].astype(F32)
        fin[rs, :] = total.astype(BF16)
        for k in range(max(a, 1), a + n):
            block = pl.ds(k * cap, cap)
            back[k] = remote(fin.at[block], ret.at[block], (flip(me, k), t))
            back[k].start()
            sent.append(back[k])
        if a == 0:
            ret[0:cap, :] = fin[0:cap, :]

    def mixer_end():
        for load in loads[3:]:
            load.wait()
        for h in range(heads):
            lanes = slice(h * HEAD_DIM, (h + 1) * HEAD_DIM)
            r = rec[:, lanes] + lax.dot_general(
                qg[:, lanes], est[h].astype(BF16), (((1,), (1,)), ((), ())),
                preferred_element_type=F32,
            )
            r = r * lax.rsqrt(jnp.mean(r * r, axis=-1, keepdims=True) + 1e-06)
            mhid[:, lanes] = (
                r * hscale_ref[:, lanes] * jax.nn.silu(o_ref[:, lanes].astype(F32))
            ).astype(BF16)
        R = mix_out.shape[0]
        wide = mixw.shape[1]
        step = min(512, wide)

        def one(i, _):
            cc = pl.ds(pl.multiple_of(i * step, step), step)
            y = jnp.dot(mhid[...], mixw[:, cc], preferred_element_type=F32).astype(BF16)
            for d in range(T):
                mpart[d % 2, d // 2, :, cc] = y[d * R:(d + 1) * R, :]
            return 0

        lax.fori_loop(0, wide // step, one, 0)
        rs_partner["m"] = remote(mpart.at[oc], mprecv, (me, 2 * g + oc))
        rs_partner["m"].start()
        sent.append(rs_partner["m"])

    def mixer_cross():
        rs_partner["m"].wait_recv()
        for j in range(1, G):
            gj = flip(g, j)
            mxsend[j - 1] = (mpart[c, gj].astype(F32) + mprecv[gj].astype(F32)).astype(BF16)
            rs_cross["m", j] = remote(mxsend.at[j - 1], mxrecv.at[j - 1], (me, 2 * gj + c))
            rs_cross["m", j].start()
            sent.append(rs_cross["m", j])

    def mixer_out():
        total = mpart[c, g].astype(F32) + mprecv[g].astype(F32)
        for j in range(1, G):
            rs_cross["m", j].wait_recv()
            total += mxrecv[j - 1].astype(F32)
        mix_out[...] = total.astype(BF16)

    last = len(pieces) - 1
    hop_next = 1
    gather_start(0)
    hop_recv(0)
    if len(hops) > 1:
        hop_send(1)
    gather_relay(0)
    for load in loads[:3]:
        load.wait()
    for p in range(len(pieces)):
        if p < last:
            gather_start(p + 1)
        gather_end(p)
        if p > 0:
            scatter_cross(p - 1)
        experts(p)
        if p < last:
            gather_relay(p + 1)
        if p > 0:
            give_back(p - 1)
        if p + 2 < len(hops) and p < last:
            hop_recv(p + 1)
            hop_send(p + 2)
            hop_next = p + 2
    scatter_cross(last)
    for r in range(hop_next, len(hops)):
        hop_recv(r)
        if r + 1 < len(hops):
            hop_send(r + 1)
    mixer_end()
    give_back(last)
    mixer_cross()
    mixer_out()
    for k in range(1, E):
        back[k].wait_recv()
    exp_out[...] = lax.dot_general(
        wmat[...], ret[...], (((0,), (0,)), ((), ())), preferred_element_type=F32
    ).astype(BF16)
    for copy in sent:
        copy.wait_send()
    for r in range(len(hops)):
        @pl.when(me + hops[r] < E)
        def _():
            hop_copy[r].wait_send()


def body(E, T, q, f, v, o, gap, extra, hscale, mixw, tok, escale, routes, scores, gate, up, down):
    tokens, width = q.shape
    ntok, D = tok.shape
    heads = width // HEAD_DIM
    G = T // 2
    cap = -(-(3 * ntok // E) // 16) * 16
    S = E * cap
    Dl = D // T
    FFl = gate.shape[2]
    R = tokens // T
    half, quarter = E // 2, E // 4
    pieces = ((0, half), (half, quarter), (half + quarter, quarter))
    nhops = max(1, (E - 1).bit_length())
    copies = 2 * (E - 1) + nhops + len(pieces) * (G - 1 + G + 1 + G - 1) + G
    vm = pl.BlockSpec(memory_space=pltpu.VMEM)
    anyspace = pl.BlockSpec(memory_space=pl.ANY)
    V = pltpu.VMEM
    scratch = [
        V((D, FFl), BF16), V((D, FFl), BF16), V((D, FFl), BF16), V(mixw.shape, BF16),
        V((ntok, Dl), BF16), V((S, ntok), BF16), V((S, ntok), BF16), V((S, Dl), BF16),
        V((T, S, Dl), BF16), V((S, FFl), BF16), V((2, G, S, Dl), BF16), V((G, S, Dl), BF16),
        V((max(G - 1, 1), S, Dl), BF16), V((max(G - 1, 1), S, Dl), BF16),
        V((S, Dl), BF16), V((S, Dl), BF16),
        V((tokens, width), F32), V((tokens, width), F32), V((tokens, width), F32),
        V((tokens, width), BF16), V((tokens, width), F32),
        V((heads, HEAD_DIM, HEAD_DIM), F32), V((heads, 16, HEAD_DIM), F32),
        V((heads, HEAD_DIM, HEAD_DIM), F32), V((heads, 16, HEAD_DIM), F32),
        V((nhops, heads, HEAD_DIM + 16, HEAD_DIM), BF16),
        V((nhops, heads, HEAD_DIM + 16, HEAD_DIM), BF16),
        V((tokens, width), BF16), V((2, G, R, D), BF16), V((G, R, D), BF16),
        V((max(G - 1, 1), R, D), BF16), V((max(G - 1, 1), R, D), BF16),
        pltpu.SemaphoreType.DMA((4,)),
        pltpu.SemaphoreType.DMA((copies,)),
        pltpu.SemaphoreType.DMA((copies,)),
    ]
    return pl.pallas_call(
        functools.partial(kernel, E, T, cap, pieces),
        out_shape=(
            jax.ShapeDtypeStruct((R, D), BF16),
            jax.ShapeDtypeStruct((ntok, Dl), BF16),
        ),
        in_specs=[vm] * 7 + [anyspace] + [vm] * 4 + [anyspace] * 3,
        out_specs=(vm, vm),
        scratch_shapes=scratch,
        compiler_params=pltpu.CompilerParams(
            collective_id=0, has_side_effects=True, vmem_limit_bytes=60 * 1024 * 1024
        ),
    )(
        q, f, v, o, gap[None], extra, hscale[None], mixw, tok, escale[None],
        routes.T, scores.T, gate[0], up[0], down[0],
    )


def solution(mesh):
    E, T = mesh.shape["ep"], mesh.shape["tp"]
    return jax.shard_map(
        functools.partial(body, E, T),
        mesh=mesh,
        in_specs=(
            P("ep", "tp"),
            P("ep", "tp"),
            P("ep", "tp"),
            P("ep", "tp"),
            P("tp"),
            P("ep", "tp"),
            P("tp"),
            P("tp", None),
            P("ep", None),
            P(),
            P("ep", None),
            P("ep", None),
            P("ep", None, "tp"),
            P("ep", None, "tp"),
            P("ep", None, "tp"),
        ),
        out_specs=(P(("ep", "tp"), None), P("ep", "tp")),
        check_vma=False,
    )
```

profile of v0, /device:TPU:11, one launch (start us, length us, event | category | flops | bytes accessed | tf_op | source)
XLA Modules:
  0.0 78.7 jit_solution(14882371348303009995)
XLA Ops:
  0.6 74.8 %shard_map.158 = (bf16[64,2048]{1,0:T(8,128)(2,1)}, bf16[256,512]{1,0:T(8,128)(2,1)}) custom-call(bf16[256,512]{1,0:T(8,128)(2,1)} %q_ref.1, bf16[256,512]{1,0:T(8,128)(2,1)} %f_ref.1, bf16[256,512]{1,0:T(8,128)(2,1)} %v_ref.1, bf16[256,512]{1,0:T(8,128)(2,1)} %o_ref.1, f32[1,512]{1,0:T(1,128)} %bitcast.12, f32[256,512]{1,0:T(8,128)} %extra_ref.1, ...), custom_call_target="tpu_custom_call" | custom-call | tf_op jit(solution)/shard_map/pallas_call | solution.py:431
  75.4 1.7 %copy.19 = bf16[64,2048]{1,0:T(8,128)(2,1)} copy(bf16[64,2048]{1,0:T(8,128)(2,1)} %get-tuple-element.4) | data formatting | bytes 524288
  77.1 1.7 %copy.20 = bf16[256,512]{1,0:T(8,128)(2,1)} copy(bf16[256,512]{1,0:T(8,128)(2,1)} %get-tuple-element.5) | data formatting | bytes 524288
where the time goes:
time: 79 us; the launch traced here: 78.7 us
  Pallas kernels  74.8 us (95%)
  local copies, waits for them, and re-layouts  3.34 us (4%)
    pallas_call x1, Pallas kernels, body(): pl.pallas_call(functools.partial(kernel, E, T, cap, pieces), out_shape=(j...  74.8 us
    unnamed x2, local copies, waits for them, and re-layouts  3.34 us

commit v1 on v0

v1 whole, which is shorter than its diff:
```python
import functools

import jax
import jax.numpy as jnp
from jax import lax
from jax.experimental import pallas as pl
from jax.experimental.pallas import tpu as pltpu
from jax.sharding import PartitionSpec as P

HEAD_DIM = 128
CHUNK = 64
MESH = pl.DeviceIdType.MESH
F32 = jnp.float32
BF16 = jnp.bfloat16


def flip(i, k):
    b = 1
    while b <= k:
        if k & b:
            i = i + b - 2 * b * lax.rem(lax.div(i, b), 2)
        b *= 2
    return i


def kernel(
    E, T, cap, near, groups, plan,
    q_hbm, f_hbm, v_hbm, o_hbm, gap_ref, extra_hbm, hscale_ref,
    mixw_hbm, tok_ref, escale_ref, routes_ref, scores_ref,
    gate_hbm, up_hbm, down_hbm,
    mix_out, exp_out,
    q_ref, f_ref, v_ref, o_ref, extra_ref,
    gate, up, down, mixw,
    ncols, dmat, wmat, outgoing, nearout, feats, hidden, part, precv, xsend, xrecv, fin, ret,
    qs, ks, run, qg, rec, ist, idec, est, bst, bdec, psum, pdec, ksend, krecv, csend, crecv,
    mhid, mpart, mprecv, mxsend, mxrecv,
    wsem, send_sem, recv_sem,
):
    me = lax.axis_index("ep")
    t = lax.axis_index("tp")
    G = T // 2
    g, c = lax.div(t, 2), lax.rem(t, 2)
    oc = 1 - c
    tokens, width = q_ref.shape
    heads = width // HEAD_DIM
    Dl = outgoing.shape[1]
    FFl = hidden.shape[1]

    loads = [
        pltpu.make_async_copy(src, dst, wsem.at[i])
        for i, (src, dst) in enumerate(
            (
                (f_hbm, f_ref), (extra_hbm, extra_ref), (q_hbm, q_ref), (v_hbm, v_ref),
                (gate_hbm, gate), (up_hbm, up), (down_hbm, down),
                (o_hbm, o_ref), (mixw_hbm, mixw),
            )
        )
    ]

    barrier = pltpu.get_barrier_semaphore()
    for k in range(1, E):
        pl.semaphore_signal(barrier, inc=1, device_id=(flip(me, k), t), device_id_type=MESH)
    pl.semaphore_signal(barrier, inc=1, device_id=(me, 2 * g + oc), device_id_type=MESH)
    for j in range(1, G):
        pl.semaphore_signal(
            barrier, inc=1, device_id=(me, 2 * flip(g, j) + c), device_id_type=MESH
        )

    for load in loads:
        load.start()

    used = [0]

    def remote(src, dst, device):
        slot = used[0]
        used[0] += 1
        return pltpu.make_async_remote_copy(
            src_ref=src, dst_ref=dst, send_sem=send_sem.at[slot], recv_sem=recv_sem.at[slot],
            device_id=device, device_id_type=MESH,
        )

    sent = []

    def launch(copy):
        copy.start()
        sent.append(copy)
        return copy

    x = tok_ref[...].astype(F32)
    mean = jnp.mean(x, axis=-1, keepdims=True)
    centred = x - mean
    inv = lax.rsqrt(jnp.mean(centred * centred, axis=-1, keepdims=True) + 1e-05)

    def normed(cols):
        return ((tok_ref[:, cols].astype(F32) - mean) * inv * escale_ref[:, cols]).astype(BF16)

    ntok = tok_ref.shape[0]
    ek = lax.broadcasted_iota(jnp.int32, (E, ntok), 0) ^ me
    first, second = routes_ref[0:1, :] == ek, routes_ref[1:2, :] == ek
    named = jnp.where(first | second, 1.0, 0.0)
    earlier = jnp.where(
        lax.broadcasted_iota(jnp.int32, (ntok, ntok), 0)
        < lax.broadcasted_iota(jnp.int32, (ntok, ntok), 1), 1.0, 0.0
    ).astype(BF16)
    position = jnp.dot(named.astype(BF16), earlier, preferred_element_type=F32)
    place = jnp.where(first | second, position, -1.0).astype(jnp.int32)
    rows = lax.broadcasted_iota(jnp.int32, (cap, ntok), 0)

    def choose(k):
        dmat[k * cap:(k + 1) * cap, :] = jnp.where(rows == place[k:k + 1, :], 1.0, 0.0).astype(BF16)

    for k in range(near, E):
        choose(k)
    own = normed(pl.ds(pl.multiple_of(t * Dl, 128), Dl))
    outgoing[...] = jnp.dot(
        dmat[near * cap:, :], own, preferred_element_type=F32
    ).astype(BF16)

    dispatch = {}
    order = [k for p in plan["far"] for k in range(groups[p][0], sum(groups[p]))]
    for k in order:
        dispatch[k] = remote(
            outgoing.at[pl.ds((k - near) * cap, cap)],
            feats.at[c, g, pl.ds(k * cap, cap)], (flip(me, k), t),
        )

    pl.semaphore_wait(barrier, E - 1 + 1 + G - 1)

    for k in order:
        launch(dispatch[k])

    for load in loads[:4]:
        load.wait()
    closing = gap_ref[...] * jax.nn.sigmoid(-f_ref[...].astype(F32))
    ks[...] = closing
    logd = jnp.log1p(-closing) + extra_ref[...]
    qs[...] = jax.nn.silu(q_ref[...].astype(F32))
    r_i = lax.broadcasted_iota(jnp.int32, (CHUNK, CHUNK), 0)
    c_i = lax.broadcasted_iota(jnp.int32, (CHUNK, CHUNK), 1)
    causal = r_i >= c_i
    tri = jnp.where(causal, 1.0, 0.0).astype(F32)
    nchunks = tokens // CHUNK
    for n in range(nchunks):
        run[n * CHUNK:(n + 1) * CHUNK, :] = jnp.dot(
            tri, logd[n * CHUNK:(n + 1) * CHUNK, :], precision=lax.Precision.HIGHEST,
            preferred_element_type=F32,
        )

    def head_local(h, _):
        lanes = pl.ds(pl.multiple_of(h * HEAD_DIM, HEAD_DIM), HEAD_DIM)
        state = jnp.zeros((HEAD_DIM, HEAD_DIM), F32)
        before = jnp.zeros((1, HEAD_DIM), F32)
        for n in range(nchunks):
            rs = slice(n * CHUNK, (n + 1) * CHUNK)
            r = run[rs, lanes]
            total = r[CHUNK - 1:CHUNK, :]
            qd = qs[rs, lanes] * jnp.exp(r)
            key = ks[rs, lanes]
            kd = (key * jnp.exp(-r)).astype(BF16)
            kst = (key * jnp.exp(total - r)).astype(BF16)
            val = v_ref[rs, lanes]
            qd_b = qd.astype(BF16)
            scores = lax.dot_general(
                qd_b, kd, (((1,), (1,)), ((), ())), preferred_element_type=F32
            )
            scores = jnp.where(causal, scores, 0.0).astype(BF16)
            out = jnp.dot(scores, val, preferred_element_type=F32)
            if n:
                out += lax.dot_general(
                    qd_b, state.astype(BF16), (((1,), (1,)), ((), ())),
                    preferred_element_type=F32,
                )
            rec[rs, lanes] = out
            qg[rs, lanes] = (qd * jnp.exp(before)).astype(BF16)
            state = state * jnp.exp(total) + lax.dot_general(
                val, kst, (((0,), (0,)), ((), ())), preferred_element_type=F32
            )
            before = before + total
        ist[h] = state
        idec[h] = jnp.broadcast_to(jnp.exp(before), (16, HEAD_DIM))
        return 0

    lax.fori_loop(0, heads, head_local, 0)

    odd = lax.rem(me, 2) == 1
    z = lax.div(me, 2)
    Z = E // 2
    ksend[:, 0:HEAD_DIM, :] = ist[...].astype(BF16)
    ksend[:, HEAD_DIM:, :] = idec[...].astype(BF16)
    pair = launch(remote(ksend, krecv, (flip(me, 1), t)))
    chain = remote(csend, crecv, (lax.rem(me + 2, E), t)) if Z > 1 else None

    def pair_end():
        pair.wait_recv()
        s = krecv[:, 0:HEAD_DIM, :].astype(F32)
        d = krecv[:, HEAD_DIM:, :].astype(F32)
        bst[...] = jnp.where(odd, s, 0.0)
        bdec[...] = jnp.where(odd, d, 1.0)
        psum[...] = jnp.where(
            odd, idec[:, 0:1, :] * s + ist[...], d[:, 0:1, :] * ist[...] + s
        )
        pdec[...] = idec[...] * d

    def chain_step(i):
        @pl.when(z == i)
        def _():
            if i:
                chain.wait_recv()
                carry = crecv[...].astype(F32)
                est[...] = bdec[:, 0:1, :] * carry + bst[...]
                if i + 1 < Z:
                    csend[...] = (pdec[:, 0:1, :] * carry + psum[...]).astype(BF16)
            else:
                est[...] = bst[...]
                if i + 1 < Z:
                    csend[...] = psum[...].astype(BF16)
            if i + 1 < Z:
                chain.start()

    for k in range(near):
        choose(k)
    for d in range(T):
        ncols[d % 2, d // 2] = normed(slice(d * Dl, (d + 1) * Dl))
    for j in range(G):
        nearout[j] = jnp.dot(
            dmat[cap:near * cap, :], ncols[c, j], preferred_element_type=F32
        ).astype(BF16)
    for k in range(1, near):
        dispatch[k] = launch(remote(
            nearout.at[:, pl.ds((k - 1) * cap, cap)],
            feats.at[c, :, pl.ds(k * cap, cap)], (flip(me, k), t),
        ))
    for d in range(T):
        feats[d % 2, d // 2, 0:cap, :] = jnp.dot(
            dmat[0:cap, :], ncols[d % 2, d // 2], preferred_element_type=F32
        ).astype(BF16)
    w0 = jax.nn.sigmoid(scores_ref[0:1, :] - scores_ref[1:2, :])
    weight = jnp.where(first, w0, jnp.where(second, 1.0 - w0, 0.0))
    for k in range(E):
        wmat[k * cap:(k + 1) * cap, :] = jnp.where(
            rows == place[k:k + 1, :], weight[k:k + 1, :], 0.0
        ).astype(BF16)

    ag_partner, ag_cross, rs_partner, rs_cross, back = {}, {}, {}, {}, {}
    partner = (me, 2 * g + oc)

    def piece_rows(p):
        a, n = groups[p]
        return pl.ds(a * cap, n * cap)

    def gather_start(p):
        a, n = groups[p]
        lo = max(a, 1)
        if lo == a + n:
            return
        for k in range(lo, a + n):
            dispatch[k].wait_recv()
        if a < near:
            rr = pl.ds(lo * cap, (a + n - lo) * cap)
            ag_partner[p, 0] = launch(remote(feats.at[c, :, rr], feats.at[c, :, rr], partner))
            return
        rr = piece_rows(p)
        for j in range(1, G):
            ag_cross[p, j] = launch(
                remote(feats.at[c, g, rr], feats.at[c, g, rr], (me, 2 * flip(g, j) + c))
            )
        ag_partner[p, 0] = launch(remote(feats.at[c, g, rr], feats.at[c, g, rr], partner))

    def gather_relay(p):
        rr = piece_rows(p)
        for j in range(1, G):
            ag_cross[p, j].wait_recv()
            gj = flip(g, j)
            ag_partner[p, j] = launch(remote(feats.at[c, gj, rr], feats.at[c, gj, rr], partner))

    def gather_end(p):
        for j in range(G):
            if (p, j) in ag_partner:
                ag_partner[p, j].wait_recv()

    tile = min(256, FFl)

    def experts(p):
        gather_end(p)
        a, n = groups[p]
        rs = slice(a * cap, (a + n) * cap)

        def one(i, _):
            cc = pl.ds(pl.multiple_of(i * tile, tile), tile)
            ga = jnp.zeros((n * cap, tile), F32)
            ua = jnp.zeros((n * cap, tile), F32)
            for d in range(T):
                xs = feats[d % 2, d // 2, rs, :]
                ga += jnp.dot(xs, gate[d * Dl:(d + 1) * Dl, cc], preferred_element_type=F32)
                ua += jnp.dot(xs, up[d * Dl:(d + 1) * Dl, cc], preferred_element_type=F32)
            hidden[rs, cc] = (jax.nn.silu(ga) * ua).astype(BF16)
            return 0

        lax.fori_loop(0, FFl // tile, one, 0)

        def down_group(cls, gg):
            ff = pl.ds(pl.multiple_of((2 * gg + cls) * Dl, 128), Dl)
            part[cls, gg, rs, :] = lax.dot_general(
                hidden[rs, :], down[ff, :], (((1,), (1,)), ((), ())),
                preferred_element_type=F32,
            ).astype(BF16)

        def theirs(gg, _):
            down_group(oc, gg)
            return 0

        def ours(gg, _):
            down_group(c, gg)
            return 0

        lax.fori_loop(0, G, theirs, 0)
        rr = piece_rows(p)
        rs_partner[p] = launch(remote(part.at[oc, :, rr], precv.at[:, rr], partner))
        lax.fori_loop(0, G, ours, 0)

    def scatter_cross(p):
        a, n = groups[p]
        rs = slice(a * cap, (a + n) * cap)
        rr = piece_rows(p)
        rs_partner[p].wait_recv()
        for j in range(1, G):
            gj = flip(g, j)
            xsend[j - 1, rs, :] = (
                part[c, gj, rs, :].astype(F32) + precv[gj, rs, :].astype(F32)
            ).astype(BF16)
            rs_cross[p, j] = launch(
                remote(xsend.at[j - 1, rr], xrecv.at[j - 1, rr], (me, 2 * gj + c))
            )

    def give_back(p):
        a, n = groups[p]
        rs = slice(a * cap, (a + n) * cap)
        total = part[c, g, rs, :].astype(F32) + precv[g, rs, :].astype(F32)
        for j in range(1, G):
            rs_cross[p, j].wait_recv()
            total += xrecv[j - 1, rs, :].astype(F32)
        fin[rs, :] = total.astype(BF16)
        for k in range(max(a, 1), a + n):
            block = pl.ds(k * cap, cap)
            back[k] = launch(remote(fin.at[block], ret.at[block], (flip(me, k), t)))
        if a == 0:
            ret[0:cap, :] = fin[0:cap, :]

    def mixer_end():
        for load in loads[7:]:
            load.wait()
        for h in range(heads):
            lanes = slice(h * HEAD_DIM, (h + 1) * HEAD_DIM)
            r = rec[:, lanes] + lax.dot_general(
                qg[:, lanes], est[h].astype(BF16), (((1,), (1,)), ((), ())),
                preferred_element_type=F32,
            )
            r = r * lax.rsqrt(jnp.mean(r * r, axis=-1, keepdims=True) + 1e-06)
            mhid[:, lanes] = (
                r * hscale_ref[:, lanes] * jax.nn.silu(o_ref[:, lanes].astype(F32))
            ).astype(BF16)
        R = mix_out.shape[0]
        wide = mixw.shape[1]
        step = min(512, wide)

        def one(i, _):
            cc = pl.ds(pl.multiple_of(i * step, step), step)
            y = jnp.dot(mhid[...], mixw[:, cc], preferred_element_type=F32).astype(BF16)
            for d in range(T):
                mpart[d % 2, d // 2, :, cc] = y[d * R:(d + 1) * R, :]
            return 0

        lax.fori_loop(0, wide // step, one, 0)
        rs_partner["m"] = launch(remote(mpart.at[oc], mprecv, partner))

    def mixer_cross():
        rs_partner["m"].wait_recv()
        for j in range(1, G):
            gj = flip(g, j)
            mxsend[j - 1] = (mpart[c, gj].astype(F32) + mprecv[gj].astype(F32)).astype(BF16)
            rs_cross["m", j] = launch(
                remote(mxsend.at[j - 1], mxrecv.at[j - 1], (me, 2 * gj + c))
            )

    def mixer_out():
        total = mpart[c, g].astype(F32) + mprecv[g].astype(F32)
        for j in range(1, G):
            rs_cross["m", j].wait_recv()
            total += mxrecv[j - 1].astype(F32)
        mix_out[...] = total.astype(BF16)

    def chain_rest():
        for i in range(plan["chain"], Z):
            chain_step(i)

    steps = {
        "a": gather_start, "b": gather_relay, "c": experts, "d": scatter_cross, "e": give_back,
        "pair": pair_end, "chain": chain_step, "chains": chain_rest,
        "mc": mixer_end, "md": mixer_cross, "me": mixer_out,
    }
    for load in loads[4:7]:
        load.wait()
    for step in plan["steps"]:
        steps[step[0]](*step[1:])
    for k in range(1, E):
        back[k].wait_recv()
    exp_out[...] = lax.dot_general(
        wmat[...], ret[...], (((0,), (0,)), ((), ())), preferred_element_type=F32
    ).astype(BF16)
    for copy in sent:
        copy.wait_send()
    if chain is not None:
        @pl.when(me + 2 < E)
        def _():
            chain.wait_send()


def make_plan(count):
    n = list(range(count // 2))
    f = list(range(count // 2, count))[::-1]
    steps = [
        "c n0", "a f0", "d n0", "pair", "chain 0", "a n1", "b f0", "a f1", "c f0", "b f1",
        "chain 1", "d f0", "a f2", "c n1", "c f1", "e n0", "e f0", "b f2", "d f1", "a f3",
        "a n2", "d n1", "chain 2", "c n2", "c f2", "e f1", "e n1", "b f3", "d f2", "a n3",
        "d n2", "chains", "c n3", "c f3", "e f2", "e n2", "d f3", "d n3", "mc", "e f3", "md",
        "e n3", "me",
    ]
    parsed = []
    for s in steps:
        name, *rest = s.split()
        where = [(n if r[0] == "n" else f)[int(r[1])] if r[0] in "nf" else int(r) for r in rest]
        parsed.append((name, *where))
    return {"far": f, "steps": parsed, "chain": 3}


def body(E, T, q, f, v, o, gap, extra, hscale, mixw, tok, escale, routes, scores, gate, up, down):
    tokens, width = q.shape
    ntok, D = tok.shape
    heads = width // HEAD_DIM
    G = T // 2
    cap = -(-(3 * ntok // E) // 16) * 16
    S = E * cap
    Dl = D // T
    FFl = gate.shape[2]
    R = tokens // T
    near = E // 2
    each = E // 8
    groups = tuple((i * each, each) for i in range(8))
    copies = 2 * (E - 1) + 2 + len(groups) * (G - 1 + G + 1 + G - 1) + G
    vm = pl.BlockSpec(memory_space=pltpu.VMEM)
    anyspace = pl.BlockSpec(memory_space=pl.ANY)
    V = pltpu.VMEM
    scratch = [
        V(q.shape, BF16), V(q.shape, BF16), V(q.shape, BF16), V(q.shape, BF16), V(q.shape, F32),
        V((D, FFl), BF16), V((D, FFl), BF16), V((D, FFl), BF16), V(mixw.shape, BF16),
        V((2, G, ntok, Dl), BF16), V((S, ntok), BF16), V((S, ntok), BF16),
        V(((E - near) * cap, Dl), BF16), V((G, (near - 1) * cap, Dl), BF16),
        V((2, G, S, Dl), BF16), V((S, FFl), BF16), V((2, G, S, Dl), BF16), V((G, S, Dl), BF16),
        V((max(G - 1, 1), S, Dl), BF16), V((max(G - 1, 1), S, Dl), BF16),
        V((S, Dl), BF16), V((S, Dl), BF16),
        V((tokens, width), F32), V((tokens, width), F32), V((tokens, width), F32),
        V((tokens, width), BF16), V((tokens, width), F32),
        V((heads, HEAD_DIM, HEAD_DIM), F32), V((heads, 16, HEAD_DIM), F32),
        V((heads, HEAD_DIM, HEAD_DIM), F32),
        V((heads, HEAD_DIM, HEAD_DIM), F32), V((heads, 16, HEAD_DIM), F32),
        V((heads, HEAD_DIM, HEAD_DIM), F32), V((heads, 16, HEAD_DIM), F32),
        V((heads, HEAD_DIM + 16, HEAD_DIM), BF16), V((heads, HEAD_DIM + 16, HEAD_DIM), BF16),
        V((heads, HEAD_DIM, HEAD_DIM), BF16), V((heads, HEAD_DIM, HEAD_DIM), BF16),
        V((tokens, width), BF16), V((2, G, R, D), BF16), V((G, R, D), BF16),
        V((max(G - 1, 1), R, D), BF16), V((max(G - 1, 1), R, D), BF16),
        pltpu.SemaphoreType.DMA((9,)),
        pltpu.SemaphoreType.DMA((copies,)),
        pltpu.SemaphoreType.DMA((copies,)),
    ]
    return pl.pallas_call(
        functools.partial(kernel, E, T, cap, near, groups, make_plan(len(groups))),
        out_shape=(
            jax.ShapeDtypeStruct((R, D), BF16),
            jax.ShapeDtypeStruct((ntok, Dl), BF16),
        ),
        in_specs=(
            [anyspace] * 4 + [vm, anyspace, vm, anyspace] + [vm] * 4 + [anyspace] * 3
        ),
        out_specs=(vm, vm),
        scratch_shapes=scratch,
        compiler_params=pltpu.CompilerParams(
            collective_id=0, has_side_effects=True, vmem_limit_bytes=60 * 1024 * 1024
        ),
    )(
        q, f, v, o, gap[None], extra, hscale[None], mixw, tok, escale[None],
        routes.T, scores.T, gate[0], up[0], down[0],
    )


def solution(mesh):
    E, T = mesh.shape["ep"], mesh.shape["tp"]
    return jax.shard_map(
        functools.partial(body, E, T),
        mesh=mesh,
        in_specs=(
            P("ep", "tp"),
            P("ep", "tp"),
            P("ep", "tp"),
            P("ep", "tp"),
            P("tp"),
            P("ep", "tp"),
            P("tp"),
            P("tp", None),
            P("ep", None),
            P(),
            P("ep", None),
            P("ep", None),
            P("ep", None, "tp"),
            P("ep", None, "tp"),
            P("ep", None, "tp"),
        ),
        out_specs=(P(("ep", "tp"), None), P("ep", "tp")),
        check_vma=False,
    )
```

time: 79 us -> 77.8 us (0.985)
  the two profiles are of different devices: /device:TPU:11 before, /device:TPU:0 now
where the time goes in v1:
time: 77.8 us; the launch traced here: 77.6 us
  Pallas kernels  73.6 us (95%)
  local copies, waits for them, and re-layouts  3.34 us (4%)
    pallas_call x1, Pallas kernels, body(): pl.pallas_call(functools.partial(kernel, E, T, cap, near, groups, make_pl...  73.6 us
    unnamed x2, local copies, waits for them, and re-layouts  3.34 us

profile of v1, /device:TPU:0, one launch (start us, length us, event | category | flops | bytes accessed | tf_op | source)
XLA Modules:
  0.0 77.6 jit_solution(15539157159459332907)
XLA Ops:
  0.6 73.6 %shard_map.158 = (bf16[64,2048]{1,0:T(8,128)(2,1)}, bf16[256,512]{1,0:T(8,128)(2,1)}) custom-call(bf16[256,512]{1,0:T(8,128)(2,1)} %q_hbm.1, bf16[256,512]{1,0:T(8,128)(2,1)} %f_hbm.1, bf16[256,512]{1,0:T(8,128)(2,1)} %v_hbm.1, bf16[256,512]{1,0:T(8,128)(2,1)} %o_hbm.1, f32[1,512]{1,0:T(1,128)} %bitcast.12, f32[256,512]{1,0:T(8,128)} %extra_hbm.1, ...), custom_call_target="tpu_custom_call" | custom-call | tf_op jit(solution)/shard_map/pallas_call | solution.py:475
  74.2 1.7 %copy.19 = bf16[64,2048]{1,0:T(8,128)(2,1)} copy(bf16[64,2048]{1,0:T(8,128)(2,1)} %get-tuple-element.4) | data formatting | bytes 524288
  75.9 1.7 %copy.20 = bf16[256,512]{1,0:T(8,128)(2,1)} copy(bf16[256,512]{1,0:T(8,128)(2,1)} %get-tuple-element.5) | data formatting | bytes 524288

commit v2 on v1

--- a/solution.py
+++ b/solution.py
@@ -24,7 +24,7 @@
 
 
 def kernel(
-    E, T, cap, near, groups, plan,
+    E, T, cap, near, slots, each, plan,
     q_hbm, f_hbm, v_hbm, o_hbm, gap_ref, extra_hbm, hscale_ref,
     mixw_hbm, tok_ref, escale_ref, routes_ref, scores_ref,
     gate_hbm, up_hbm, down_hbm,
@@ -106,45 +106,61 @@
     place = jnp.where(first | second, position, -1.0).astype(jnp.int32)
     rows = lax.broadcasted_iota(jnp.int32, (cap, ntok), 0)
 
-    def choose(k):
-        dmat[k * cap:(k + 1) * cap, :] = jnp.where(rows == place[k:k + 1, :], 1.0, 0.0).astype(BF16)
-
-    for k in range(near, E):
-        choose(k)
+    def choose(i):
+        k = slots[i]
+        dmat[i * cap:(i + 1) * cap, :] = jnp.where(rows == place[k:k + 1, :], 1.0, 0.0).astype(BF16)
+
+    for i in range(near, E):
+        choose(i)
     own = normed(pl.ds(pl.multiple_of(t * Dl, 128), Dl))
     outgoing[...] = jnp.dot(
         dmat[near * cap:, :], own, preferred_element_type=F32
     ).astype(BF16)
 
     dispatch = {}
-    order = [k for p in plan["far"] for k in range(groups[p][0], sum(groups[p]))]
-    for k in order:
-        dispatch[k] = remote(
-            outgoing.at[pl.ds((k - near) * cap, cap)],
-            feats.at[c, g, pl.ds(k * cap, cap)], (flip(me, k), t),
-        )
+
+    def send_far(i):
+        dispatch[i] = launch(remote(
+            outgoing.at[pl.ds((i - near) * cap, cap)],
+            feats.at[c, g, pl.ds(i * cap, cap)], (flip(me, slots[i]), t),
+        ))
+
+    def send_near(i):
+        dispatch[i] = launch(remote(
+            nearout.at[:, pl.ds((i - 1) * cap, cap)],
+            feats.at[c, :, pl.ds(i * cap, cap)], (flip(me, slots[i]), t),
+        ))
 
     pl.semaphore_wait(barrier, E - 1 + 1 + G - 1)
 
-    for k in order:
-        launch(dispatch[k])
-
-    for load in loads[:4]:
-        load.wait()
-    closing = gap_ref[...] * jax.nn.sigmoid(-f_ref[...].astype(F32))
-    ks[...] = closing
-    logd = jnp.log1p(-closing) + extra_ref[...]
-    qs[...] = jax.nn.silu(q_ref[...].astype(F32))
+    def far_out(p):
+        for i in range(p * each, (p + 1) * each):
+            send_far(i)
+
+    def near_out(p):
+        for i in range(max(1, p * each), (p + 1) * each):
+            send_near(i)
+
+    def near_prepare():
+        for i in range(near):
+            choose(i)
+        for d in range(T):
+            ncols[d % 2, d // 2] = normed(slice(d * Dl, (d + 1) * Dl))
+        for j in range(G):
+            nearout[j] = jnp.dot(
+                dmat[cap:near * cap, :], ncols[c, j], preferred_element_type=F32
+            ).astype(BF16)
+
+    def local_features():
+        for d in range(T):
+            feats[d % 2, d // 2, 0:cap, :] = jnp.dot(
+                dmat[0:cap, :], ncols[d % 2, d // 2], preferred_element_type=F32
+            ).astype(BF16)
+
     r_i = lax.broadcasted_iota(jnp.int32, (CHUNK, CHUNK), 0)
     c_i = lax.broadcasted_iota(jnp.int32, (CHUNK, CHUNK), 1)
     causal = r_i >= c_i
-    tri = jnp.where(causal, 1.0, 0.0).astype(F32)
     nchunks = tokens // CHUNK
-    for n in range(nchunks):
-        run[n * CHUNK:(n + 1) * CHUNK, :] = jnp.dot(
-            tri, logd[n * CHUNK:(n + 1) * CHUNK, :], precision=lax.Precision.HIGHEST,
-            preferred_element_type=F32,
-        )
 
     def head_local(h, _):
         lanes = pl.ds(pl.multiple_of(h * HEAD_DIM, HEAD_DIM), HEAD_DIM)
@@ -180,15 +196,30 @@
         idec[h] = jnp.broadcast_to(jnp.exp(before), (16, HEAD_DIM))
         return 0
 
-    lax.fori_loop(0, heads, head_local, 0)
-
     odd = lax.rem(me, 2) == 1
     z = lax.div(me, 2)
     Z = E // 2
-    ksend[:, 0:HEAD_DIM, :] = ist[...].astype(BF16)
-    ksend[:, HEAD_DIM:, :] = idec[...].astype(BF16)
-    pair = launch(remote(ksend, krecv, (flip(me, 1), t)))
+    pair = remote(ksend, krecv, (flip(me, 1), t))
     chain = remote(csend, crecv, (lax.rem(me + 2, E), t)) if Z > 1 else None
+
+    def recurrence():
+        for load in loads[:4]:
+            load.wait()
+        closing = gap_ref[...] * jax.nn.sigmoid(-f_ref[...].astype(F32))
+        ks[...] = closing
+        logd = jnp.log1p(-closing) + extra_ref[...]
+        qs[...] = jax.nn.silu(q_ref[...].astype(F32))
+        tri = jnp.where(causal, 1.0, 0.0).astype(F32)
+        for n in range(nchunks):
+            run[n * CHUNK:(n + 1) * CHUNK, :] = jnp.dot(
+                tri, logd[n * CHUNK:(n + 1) * CHUNK, :], precision=lax.Precision.HIGHEST,
+                preferred_element_type=F32,
+            )
+
+        lax.fori_loop(0, heads, head_local, 0)
+        ksend[:, 0:HEAD_DIM, :] = ist[...].astype(BF16)
+        ksend[:, HEAD_DIM:, :] = idec[...].astype(BF16)
+        launch(pair)
 
     def pair_end():
         pair.wait_recv()
@@ -217,44 +248,31 @@
             if i + 1 < Z:
                 chain.start()
 
-    for k in range(near):
-        choose(k)
-    for d in range(T):
-        ncols[d % 2, d // 2] = normed(slice(d * Dl, (d + 1) * Dl))
-    for j in range(G):
-        nearout[j] = jnp.dot(
-            dmat[cap:near * cap, :], ncols[c, j], preferred_element_type=F32
-        ).astype(BF16)
-    for k in range(1, near):
-        dispatch[k] = launch(remote(
-            nearout.at[:, pl.ds((k - 1) * cap, cap)],
-            feats.at[c, :, pl.ds(k * cap, cap)], (flip(me, k), t),
-        ))
-    for d in range(T):
-        feats[d % 2, d // 2, 0:cap, :] = jnp.dot(
-            dmat[0:cap, :], ncols[d % 2, d // 2], preferred_element_type=F32
-        ).astype(BF16)
-    w0 = jax.nn.sigmoid(scores_ref[0:1, :] - scores_ref[1:2, :])
-    weight = jnp.where(first, w0, jnp.where(second, 1.0 - w0, 0.0))
-    for k in range(E):
-        wmat[k * cap:(k + 1) * cap, :] = jnp.where(
-            rows == place[k:k + 1, :], weight[k:k + 1, :], 0.0
-        ).astype(BF16)
+    def weigh():
+        w0 = jax.nn.sigmoid(scores_ref[0:1, :] - scores_ref[1:2, :])
+        weight = jnp.where(first, w0, jnp.where(second, 1.0 - w0, 0.0))
+        for i in range(E):
+            k = slots[i]
+            wmat[i * cap:(i + 1) * cap, :] = jnp.where(
+                rows == place[k:k + 1, :], weight[k:k + 1, :], 0.0
+            ).astype(BF16)
 
     ag_partner, ag_cross, rs_partner, rs_cross, back = {}, {}, {}, {}, {}
     partner = (me, 2 * g + oc)
 
+    def unit(p):
+        return p * each, each
+
     def piece_rows(p):
-        a, n = groups[p]
-        return pl.ds(a * cap, n * cap)
+        return pl.ds(p * each * cap, each * cap)
 
     def gather_start(p):
-        a, n = groups[p]
+        a, n = unit(p)
         lo = max(a, 1)
         if lo == a + n:
             return
-        for k in range(lo, a + n):
-            dispatch[k].wait_recv()
+        for i in range(lo, a + n):
+            dispatch[i].wait_recv()
         if a < near:
             rr = pl.ds(lo * cap, (a + n - lo) * cap)
             ag_partner[p, 0] = launch(remote(feats.at[c, :, rr], feats.at[c, :, rr], partner))
@@ -280,13 +298,16 @@
 
     tile = min(256, FFl)
 
-    def experts(p):
-        gather_end(p)
-        a, n = groups[p]
-        rs = slice(a * cap, (a + n) * cap)
-
-        def one(i, _):
-            cc = pl.ds(pl.multiple_of(i * tile, tile), tile)
+    def experts(*units):
+        if not rs_partner:
+            for load in loads[4:7]:
+                load.wait()
+        for p in units:
+            gather_end(p)
+        n = len(units) * each
+        rs = slice(units[0] * each * cap, (units[-1] + 1) * each * cap)
+        for i in range(FFl // tile):
+            cc = slice(i * tile, (i + 1) * tile)
             ga = jnp.zeros((n * cap, tile), F32)
             ua = jnp.zeros((n * cap, tile), F32)
             for d in range(T):
@@ -294,9 +315,6 @@
                 ga += jnp.dot(xs, gate[d * Dl:(d + 1) * Dl, cc], preferred_element_type=F32)
                 ua += jnp.dot(xs, up[d * Dl:(d + 1) * Dl, cc], preferred_element_type=F32)
             hidden[rs, cc] = (jax.nn.silu(ga) * ua).astype(BF16)
-            return 0
-
-        lax.fori_loop(0, FFl // tile, one, 0)
 
         def down_group(cls, gg):
             ff = pl.ds(pl.multiple_of((2 * gg + cls) * Dl, 128), Dl)
@@ -305,21 +323,16 @@
                 preferred_element_type=F32,
             ).astype(BF16)
 
-        def theirs(gg, _):
+        for gg in range(G):
             down_group(oc, gg)
-            return 0
-
-        def ours(gg, _):
+        for p in units:
+            rr = piece_rows(p)
+            rs_partner[p] = launch(remote(part.at[oc, :, rr], precv.at[:, rr], partner))
+        for gg in range(G):
             down_group(c, gg)
-            return 0
-
-        lax.fori_loop(0, G, theirs, 0)
-        rr = piece_rows(p)
-        rs_partner[p] = launch(remote(part.at[oc, :, rr], precv.at[:, rr], partner))
-        lax.fori_loop(0, G, ours, 0)
 
     def scatter_cross(p):
-        a, n = groups[p]
+        a, n = unit(p)
         rs = slice(a * cap, (a + n) * cap)
         rr = piece_rows(p)
         rs_partner[p].wait_recv()
@@ -333,16 +346,16 @@
             )
 
     def give_back(p):
-        a, n = groups[p]
+        a, n = unit(p)
         rs = slice(a * cap, (a + n) * cap)
         total = part[c, g, rs, :].astype(F32) + precv[g, rs, :].astype(F32)
         for j in range(1, G):
             rs_cross[p, j].wait_recv()
             total += xrecv[j - 1, rs, :].astype(F32)
         fin[rs, :] = total.astype(BF16)
-        for k in range(max(a, 1), a + n):
-            block = pl.ds(k * cap, cap)
-            back[k] = launch(remote(fin.at[block], ret.at[block], (flip(me, k), t)))
+        for i in range(max(a, 1), a + n):
+            block = pl.ds(i * cap, cap)
+            back[i] = launch(remote(fin.at[block], ret.at[block], (flip(me, slots[i]), t)))
         if a == 0:
             ret[0:cap, :] = fin[0:cap, :]
 
@@ -389,18 +402,17 @@
             total += mxrecv[j - 1].astype(F32)
         mix_out[...] = total.astype(BF16)
 
-    def chain_rest():
-        for i in range(plan["chain"], Z):
+    def chain_rest(i):
+        for i in range(i, Z):
             chain_step(i)
 
     steps = {
+        "f": far_out, "n": near_out, "p": near_prepare, "l": local_features, "h": recurrence,
         "a": gather_start, "b": gather_relay, "c": experts, "d": scatter_cross, "e": give_back,
         "pair": pair_end, "chain": chain_step, "chains": chain_rest,
-        "mc": mixer_end, "md": mixer_cross, "me": mixer_out,
+        "w": weigh, "mc": mixer_end, "md": mixer_cross, "me": mixer_out,
     }
-    for load in loads[4:7]:
-        load.wait()
-    for step in plan["steps"]:
+    for step in plan:
         steps[step[0]](*step[1:])
     for k in range(1, E):
         back[k].wait_recv()
@@ -415,22 +427,18 @@
             chain.wait_send()
 
 
-def make_plan(count):
-    n = list(range(count // 2))
-    f = list(range(count // 2, count))[::-1]
-    steps = [
-        "c n0", "a f0", "d n0", "pair", "chain 0", "a n1", "b f0", "a f1", "c f0", "b f1",
-        "chain 1", "d f0", "a f2", "c n1", "c f1", "e n0", "e f0", "b f2", "d f1", "a f3",
-        "a n2", "d n1", "chain 2", "c n2", "c f2", "e f1", "e n1", "b f3", "d f2", "a n3",
-        "d n2", "chains", "c n3", "c f3", "e f2", "e n2", "d f3", "d n3", "mc", "e f3", "md",
-        "e n3", "me",
-    ]
-    parsed = []
-    for s in steps:
-        name, *rest = s.split()
-        where = [(n if r[0] == "n" else f)[int(r[1])] if r[0] in "nf" else int(r) for r in rest]
-        parsed.append((name, *where))
-    return {"far": f, "steps": parsed, "chain": 3}
+STEPS = (
+    "f 4", "f 5", "p", "n 1", "h", "f 6", "f 7", "n 2", "l", "c 0", "a 1", "a 4",
+    "d 0", "n 3", "c 1", "a 5", "b 4", "a 6", "d 1",
+    "c 4", "b 5", "d 4", "a 7", "pair", "chain 0", "c 5", "b 6", "e 0", "d 5", "a 2", "e 1",
+    "c 6", "b 7", "e 4", "a 3", "d 6", "chain 1", "c 7",
+    "e 5", "d 7", "c 2 3", "chain 2", "e 6", "d 2", "d 3", "chains 3", "mc", "e 7", "md", "w",
+    "e 2", "e 3", "me",
+)
+
+
+def make_plan():
+    return [(s[0], *(int(i) for i in s[1:])) for s in map(str.split, STEPS)]
 
 
 def body(E, T, q, f, v, o, gap, extra, hscale, mixw, tok, escale, routes, scores, gate, up, down):
@@ -445,8 +453,9 @@
     R = tokens // T
     near = E // 2
     each = E // 8
-    groups = tuple((i * each, each) for i in range(8))
-    copies = 2 * (E - 1) + 2 + len(groups) * (G - 1 + G + 1 + G - 1) + G
+    far = list(range(near, E))[::-1]
+    slots = list(range(near)) + far[1::2] + far[0::2]
+    copies = 2 * (E - 1) + 2 + 8 * (G - 1 + G + 1 + G - 1) + G
     vm = pl.BlockSpec(memory_space=pltpu.VMEM)
     anyspace = pl.BlockSpec(memory_space=pl.ANY)
     V = pltpu.VMEM
@@ -473,7 +482,7 @@
         pltpu.SemaphoreType.DMA((copies,)),
     ]
     return pl.pallas_call(
-        functools.partial(kernel, E, T, cap, near, groups, make_plan(len(groups))),
+        functools.partial(kernel, E, T, cap, near, slots, each, make_plan()),
         out_shape=(
             jax.ShapeDtypeStruct((R, D), BF16),
             jax.ShapeDtypeStruct((ntok, Dl), BF16),

time: 77.8 us -> 72 us (0.925)
  the two profiles are of different devices: /device:TPU:0 before, /device:TPU:25 now
where the time goes in v2:
time: 72 us; the launch traced here: 71.8 us
  Pallas kernels  67.8 us (94%)
  local copies, waits for them, and re-layouts  3.34 us (5%)
    pallas_call x1, Pallas kernels, body(): pl.pallas_call(functools.partial(kernel, E, T, cap, near, slots, each, ma...  67.8 us
    unnamed x2, local copies, waits for them, and re-layouts  3.34 us

profile of v2, /device:TPU:25, one launch (start us, length us, event | category | flops | bytes accessed | tf_op | source)
XLA Modules:
  0.0 71.8 jit_solution(10233449535843558678)
XLA Ops:
  0.6 67.8 %shard_map.158 = (bf16[64,2048]{1,0:T(8,128)(2,1)}, bf16[256,512]{1,0:T(8,128)(2,1)}) custom-call(bf16[256,512]{1,0:T(8,128)(2,1)} %q_hbm.1, bf16[256,512]{1,0:T(8,128)(2,1)} %f_hbm.1, bf16[256,512]{1,0:T(8,128)(2,1)} %v_hbm.1, bf16[256,512]{1,0:T(8,128)(2,1)} %o_hbm.1, f32[1,512]{1,0:T(1,128)} %bitcast.12, f32[256,512]{1,0:T(8,128)} %extra_hbm.1, ...), custom_call_target="tpu_custom_call" | custom-call | tf_op jit(solution)/shard_map/pallas_call | solution.py:484
  68.4 1.7 %copy.19 = bf16[64,2048]{1,0:T(8,128)(2,1)} copy(bf16[64,2048]{1,0:T(8,128)(2,1)} %get-tuple-element.4) | data formatting | bytes 524288
  70.1 1.7 %copy.20 = bf16[256,512]{1,0:T(8,128)(2,1)} copy(bf16[256,512]{1,0:T(8,128)(2,1)} %get-tuple-element.5) | data formatting | bytes 524288

commit v3 on v2

--- a/solution.py
+++ b/solution.py
@@ -428,12 +428,12 @@
 
 
 STEPS = (
-    "f 4", "f 5", "p", "n 1", "h", "f 6", "f 7", "n 2", "l", "c 0", "a 1", "a 4",
-    "d 0", "n 3", "c 1", "a 5", "b 4", "a 6", "d 1",
-    "c 4", "b 5", "d 4", "a 7", "pair", "chain 0", "c 5", "b 6", "e 0", "d 5", "a 2", "e 1",
-    "c 6", "b 7", "e 4", "a 3", "d 6", "chain 1", "c 7",
-    "e 5", "d 7", "c 2 3", "chain 2", "e 6", "d 2", "d 3", "chains 3", "mc", "e 7", "md", "w",
-    "e 2", "e 3", "me",
+    "f 4", "f 5", "p", "n 1", "n 2", "h", "f 6", "f 7", "n 3", "l", "c 0", "a 1",
+    "d 0", "c 1", "a 4", "a 2", "pair", "chain 0", "a 5", "d 1", "c 2", "b 4", "b 5", "a 6",
+    "a 7",
+    "c 4 5", "e 0", "chain 1", "e 1", "d 4", "d 5", "d 2", "a 3", "c 3", "b 6", "b 7", "chain 2",
+    "e 4", "c 6 7", "e 5", "d 6", "d 7", "d 3", "e 2", "chains 3", "mc", "e 6", "md", "e 7",
+    "w", "e 3", "me",
 )
 
 

time: 72 us -> 60.7 us (0.84)
  the two profiles are of different devices: /device:TPU:25 before, /device:TPU:0 now
where the time goes in v3:
time: 60.7 us; the launch traced here: 60.5 us
  Pallas kernels  56.5 us (93%)
  local copies, waits for them, and re-layouts  3.34 us (6%)
  between operations  0.65 us (1%)
    pallas_call x1, Pallas kernels, body(): pl.pallas_call(functools.partial(kernel, E, T, cap, near, slots, each, ma...  56.5 us
    unnamed x2, local copies, waits for them, and re-layouts  3.34 us

profile of v3, /device:TPU:0, one launch (start us, length us, event | category | flops | bytes accessed | tf_op | source)
XLA Modules:
  0.0 60.5 jit_solution(6704906576162649276)
XLA Ops:
  0.6 56.5 %shard_map.158 = (bf16[64,2048]{1,0:T(8,128)(2,1)}, bf16[256,512]{1,0:T(8,128)(2,1)}) custom-call(bf16[256,512]{1,0:T(8,128)(2,1)} %q_hbm.1, bf16[256,512]{1,0:T(8,128)(2,1)} %f_hbm.1, bf16[256,512]{1,0:T(8,128)(2,1)} %v_hbm.1, bf16[256,512]{1,0:T(8,128)(2,1)} %o_hbm.1, f32[1,512]{1,0:T(1,128)} %bitcast.12, f32[256,512]{1,0:T(8,128)} %extra_hbm.1, ...), custom_call_target="tpu_custom_call" | custom-call | tf_op jit(solution)/shard_map/pallas_call | solution.py:484
  57.1 1.7 %copy.19 = bf16[64,2048]{1,0:T(8,128)(2,1)} copy(bf16[64,2048]{1,0:T(8,128)(2,1)} %get-tuple-element.4) | data formatting | bytes 524288
  58.8 1.7 %copy.20 = bf16[256,512]{1,0:T(8,128)(2,1)} copy(bf16[256,512]{1,0:T(8,128)(2,1)} %get-tuple-element.5) | data formatting | bytes 524288

commit v4 on v3

--- a/solution.py
+++ b/solution.py
@@ -32,7 +32,7 @@
     q_ref, f_ref, v_ref, o_ref, extra_ref,
     gate, up, down, mixw,
     ncols, dmat, wmat, outgoing, nearout, feats, hidden, part, precv, xsend, xrecv, fin, ret,
-    qs, ks, run, qg, rec, ist, idec, est, bst, bdec, psum, pdec, ksend, krecv, csend, crecv,
+    qs, ks, run, qg, rec, ist, idec, est, bst, bdec, psum, pdec, ksend, krecv, csend, crecv, tsend, trecv,
     mhid, mpart, mprecv, mxsend, mxrecv,
     wsem, send_sem, recv_sem,
 ):
@@ -80,6 +80,7 @@
         )
 
     sent = []
+    partner = (me, 2 * g + oc)
 
     def launch(copy):
         copy.start()
@@ -106,9 +107,27 @@
     place = jnp.where(first | second, position, -1.0).astype(jnp.int32)
     rows = lax.broadcasted_iota(jnp.int32, (cap, ntok), 0)
 
+    z = lax.div(me, 2)
+    Z = E // 2
+    swap = E == 8
+    inner = lax.rem(z + lax.div(z, 2), 2) if swap else 0
+
+    def by_side(a, b):
+        return a + inner * (b - a)
+
+    def peer(a, b):
+        return flip(me, a) if a == b else by_side(flip(me, a), flip(me, b))
+
+    def row_of(table, i):
+        a, b = (to[i] for to in slots["to"])
+        outside, inside = table[a:a + 1, :], table[b:b + 1, :]
+        return outside if a == b else jnp.where(inner == 1, inside, outside)
+
+    def cross(i):
+        return (i - near) % 2 if swap else 0
+
     def choose(i):
-        k = slots[i]
-        dmat[i * cap:(i + 1) * cap, :] = jnp.where(rows == place[k:k + 1, :], 1.0, 0.0).astype(BF16)
+        dmat[i * cap:(i + 1) * cap, :] = jnp.where(rows == row_of(place, i), 1.0, 0.0).astype(BF16)
 
     for i in range(near, E):
         choose(i)
@@ -119,16 +138,45 @@
 
     dispatch = {}
 
+    far_base, back_base = used[0], used[0] + E
+    used[0] += 2 * E
+
+    def placed(src, dst, position, device, send, base):
+        block = pl.ds(pl.multiple_of(position * cap, 16), cap)
+        return pltpu.make_async_remote_copy(
+            src_ref=src, dst_ref=dst(block), send_sem=send_sem.at[base + send],
+            recv_sem=recv_sem.at[base + position], device_id=device, device_id_type=MESH,
+        )
+
+    def far_block(block):
+        return feats.at[c, g, block]
+
+    def ret_block(block):
+        return ret.at[block]
+
     def send_far(i):
-        dispatch[i] = launch(remote(
-            outgoing.at[pl.ds((i - near) * cap, cap)],
-            feats.at[c, g, pl.ds(i * cap, cap)], (flip(me, slots[i]), t),
-        ))
+        a, b = (to[i] for to in slots["to"])
+        to = near + 2 * inner + (i - near) // 2 if swap else i
+        src = outgoing.at[pl.ds((i - near) * cap, cap)]
+        launch(placed(src, far_block, to, (peer(a, b), t), i, far_base))
+
+    def far_arrived(i):
+        src = outgoing.at[pl.ds((i - near) * cap, cap)]
+        placed(src, far_block, i, partner, i, far_base).wait_recv()
+
+    def send_back(i):
+        a, b = (source[i] for source in slots["from"])
+        to = near + inner + 2 * cross(i) if swap and i >= near else i
+        src = fin.at[pl.ds(i * cap, cap)]
+        launch(placed(src, ret_block, to, (peer(a, b), t), i, back_base))
+
+    def back_arrived(i):
+        placed(fin.at[pl.ds(i * cap, cap)], ret_block, i, partner, i, back_base).wait_recv()
 
     def send_near(i):
         dispatch[i] = launch(remote(
             nearout.at[:, pl.ds((i - 1) * cap, cap)],
-            feats.at[c, :, pl.ds(i * cap, cap)], (flip(me, slots[i]), t),
+            feats.at[c, :, pl.ds(i * cap, cap)], (flip(me, i), t),
         ))
 
     pl.semaphore_wait(barrier, E - 1 + 1 + G - 1)
@@ -197,10 +245,12 @@
         return 0
 
     odd = lax.rem(me, 2) == 1
-    z = lax.div(me, 2)
-    Z = E // 2
     pair = remote(ksend, krecv, (flip(me, 1), t))
-    chain = remote(csend, crecv, (lax.rem(me + 2, E), t)) if Z > 1 else None
+    scan = E == 8
+    if scan:
+        climb = remote(tsend, trecv, (lax.rem(me + 2, E), t))
+        hand = [remote(csend, crecv, (lax.rem(me + 2 + 2 * i, E), t)) for i in range(2)]
+    chain = remote(csend, crecv, (lax.rem(me + 2, E), t)) if Z > 1 and not scan else None
 
     def recurrence():
         for load in loads[:4]:
@@ -232,7 +282,46 @@
         )
         pdec[...] = idec[...] * d
 
+    def carry_in(carry):
+        est[...] = bdec[:, 0:1, :] * carry + bst[...]
+
+    def scan_step(i):
+        if i == 0:
+            @pl.when(lax.rem(z, 2) == 0)
+            def _():
+                est[...] = bst[...]
+                tsend[:, 0:HEAD_DIM, :] = psum[...].astype(BF16)
+                tsend[:, HEAD_DIM:, :] = pdec[...].astype(BF16)
+                climb.start()
+        elif i == 1:
+            @pl.when(lax.rem(z, 2) == 1)
+            def _():
+                climb.wait_recv()
+
+            @pl.when(z == 1)
+            def _():
+                carry = trecv[:, 0:HEAD_DIM, :].astype(F32)
+                carry_in(carry)
+                csend[...] = (pdec[:, 0:1, :] * carry + psum[...]).astype(BF16)
+                hand[0].start()
+                hand[1].start()
+        elif i == 2:
+            @pl.when(z == 2)
+            def _():
+                hand[0].wait_recv()
+                carry_in(crecv[...].astype(F32))
+
+            @pl.when(z == 3)
+            def _():
+                hand[1].wait_recv()
+                decay = trecv[:, HEAD_DIM:HEAD_DIM + 1, :].astype(F32)
+                carry_in(decay * crecv[...].astype(F32) + trecv[:, 0:HEAD_DIM, :].astype(F32))
+
     def chain_step(i):
+        if scan:
+            scan_step(i)
+            return
+
         @pl.when(z == i)
         def _():
             if i:
@@ -252,13 +341,11 @@
         w0 = jax.nn.sigmoid(scores_ref[0:1, :] - scores_ref[1:2, :])
         weight = jnp.where(first, w0, jnp.where(second, 1.0 - w0, 0.0))
         for i in range(E):
-            k = slots[i]
             wmat[i * cap:(i + 1) * cap, :] = jnp.where(
-                rows == place[k:k + 1, :], weight[k:k + 1, :], 0.0
+                rows == row_of(place, i), row_of(weight, i), 0.0
             ).astype(BF16)
 
-    ag_partner, ag_cross, rs_partner, rs_cross, back = {}, {}, {}, {}, {}
-    partner = (me, 2 * g + oc)
+    ag_partner, ag_cross, rs_partner, rs_cross = {}, {}, {}, {}
 
     def unit(p):
         return p * each, each
@@ -272,7 +359,7 @@
         if lo == a + n:
             return
         for i in range(lo, a + n):
-            dispatch[i].wait_recv()
+            dispatch[i].wait_recv() if i < near else far_arrived(i)
         if a < near:
             rr = pl.ds(lo * cap, (a + n - lo) * cap)
             ag_partner[p, 0] = launch(remote(feats.at[c, :, rr], feats.at[c, :, rr], partner))
@@ -354,8 +441,7 @@
             total += xrecv[j - 1, rs, :].astype(F32)
         fin[rs, :] = total.astype(BF16)
         for i in range(max(a, 1), a + n):
-            block = pl.ds(i * cap, cap)
-            back[i] = launch(remote(fin.at[block], ret.at[block], (flip(me, slots[i]), t)))
+            send_back(i)
         if a == 0:
             ret[0:cap, :] = fin[0:cap, :]
 
@@ -414,13 +500,23 @@
     }
     for step in plan:
         steps[step[0]](*step[1:])
-    for k in range(1, E):
-        back[k].wait_recv()
+    for i in range(1, E):
+        back_arrived(i)
     exp_out[...] = lax.dot_general(
         wmat[...], ret[...], (((0,), (0,)), ((), ())), preferred_element_type=F32
     ).astype(BF16)
     for copy in sent:
         copy.wait_send()
+    if scan:
+        @pl.when(lax.rem(z, 2) == 0)
+        def _():
+            climb.wait_send()
+
+        @pl.when(z == 1)
+        def _():
+            hand[0].wait_send()
+            hand[1].wait_send()
+
     if chain is not None:
         @pl.when(me + 2 < E)
         def _():
@@ -428,12 +524,12 @@
 
 
 STEPS = (
-    "f 4", "f 5", "p", "n 1", "n 2", "h", "f 6", "f 7", "n 3", "l", "c 0", "a 1",
-    "d 0", "c 1", "a 4", "a 2", "pair", "chain 0", "a 5", "d 1", "c 2", "b 4", "b 5", "a 6",
-    "a 7",
-    "c 4 5", "e 0", "chain 1", "e 1", "d 4", "d 5", "d 2", "a 3", "c 3", "b 6", "b 7", "chain 2",
-    "e 4", "c 6 7", "e 5", "d 6", "d 7", "d 3", "e 2", "chains 3", "mc", "e 6", "md", "e 7",
-    "w", "e 3", "me",
+    "f 4", "f 5", "f 6", "f 7", "p", "n 1", "h", "n 2", "l", "c 0", "a 4", "d 0",
+    "a 1", "c 1", "a 5", "b 4", "pair", "chain 0", "n 3", "d 1", "c 4", "b 5", "a 2", "a 6",
+    "d 4", "chain 1", "a 7",
+    "c 5", "d 5", "a 3", "e 0", "e 1", "c 2 3", "d 2", "d 3", "e 4", "chain 2", "b 6", "b 7",
+    "c 6 7", "d 6", "d 7", "e 5", "chains 3", "mc", "e 2", "e 6", "md", "e 7", "w", "e 3",
+    "me",
 )
 
 
@@ -453,9 +549,13 @@
     R = tokens // T
     near = E // 2
     each = E // 8
-    far = list(range(near, E))[::-1]
-    slots = list(range(near)) + far[1::2] + far[0::2]
-    copies = 2 * (E - 1) + 2 + 8 * (G - 1 + G + 1 + G - 1) + G
+    close, far = list(range(near)), list(range(near, E))
+    plain = (close + far, close + far)
+    slots = {"to": plain, "from": plain}
+    if E == 8:
+        slots["to"] = (close + [6, 4, 7, 5], close + [4, 6, 5, 7])
+        slots["from"] = (close + [6, 7, 4, 5], close + [4, 5, 6, 7])
+    copies = 3 * E + 4 + 8 * (G - 1 + G + 1 + G - 1) + G
     vm = pl.BlockSpec(memory_space=pltpu.VMEM)
     anyspace = pl.BlockSpec(memory_space=pl.ANY)
     V = pltpu.VMEM
@@ -475,6 +575,7 @@
         V((heads, HEAD_DIM, HEAD_DIM), F32), V((heads, 16, HEAD_DIM), F32),
         V((heads, HEAD_DIM + 16, HEAD_DIM), BF16), V((heads, HEAD_DIM + 16, HEAD_DIM), BF16),
         V((heads, HEAD_DIM, HEAD_DIM), BF16), V((heads, HEAD_DIM, HEAD_DIM), BF16),
+        V((heads, HEAD_DIM + 16, HEAD_DIM), BF16), V((heads, HEAD_DIM + 16, HEAD_DIM), BF16),
         V((tokens, width), BF16), V((2, G, R, D), BF16), V((G, R, D), BF16),
         V((max(G - 1, 1), R, D), BF16), V((max(G - 1, 1), R, D), BF16),
         pltpu.SemaphoreType.DMA((9,)),
@@ -484,8 +585,8 @@
     return pl.pallas_call(
         functools.partial(kernel, E, T, cap, near, slots, each, make_plan()),
         out_shape=(
-            jax.ShapeDtypeStruct((R, D), BF16),
-            jax.ShapeDtypeStruct((ntok, Dl), BF16),
+            pltpu.VMEM((R, D), BF16),
+            pltpu.VMEM((ntok, Dl), BF16),
         ),
         in_specs=(
             [anyspace] * 4 + [vm, anyspace, vm, anyspace] + [vm] * 4 + [anyspace] * 3

time: 60.7 us -> 58.8 us (0.969)
  the two profiles are of different devices: /device:TPU:0 before, /device:TPU:9 now
where the time goes in v4:
time: 58.8 us; the launch traced here: 58.6 us
  Pallas kernels  56.6 us (96%)
  local copies, waits for them, and re-layouts  1.41 us (2%)
  between operations  0.65 us (1%)
    pallas_call x1, Pallas kernels, body(): pl.pallas_call(functools.partial(kernel, E, T, cap, near, slots, each, ma...  56.6 us
    unnamed x2, local copies, waits for them, and re-layouts  1.41 us

profile of v4, /device:TPU:9, one launch (start us, length us, event | category | flops | bytes accessed | tf_op | source)
XLA Modules:
  0.0 58.6 jit_solution(1172990990744689132)
XLA Ops:
  0.6 56.6 %shard_map.158 = (bf16[64,2048]{1,0:T(8,128)(2,1)S(1)}, bf16[256,512]{1,0:T(8,128)(2,1)S(1)}) custom-call(bf16[256,512]{1,0:T(8,128)(2,1)} %q_hbm.1, bf16[256,512]{1,0:T(8,128)(2,1)} %f_hbm.1, bf16[256,512]{1,0:T(8,128)(2,1)} %v_hbm.1, bf16[256,512]{1,0:T(8,128)(2,1)} %o_hbm.1, f32[1,512]{1,0:T(1,128)} %bitcast.12, f32[256,512]{1,0:T(8,128)} %extra_hbm.1, ...), custom_call_target="tpu_custom_call" | custom-call | tf_op jit(solution)/shard_map/pallas_call | solution.py:585
  57.2 0.7 %copy.19 = bf16[64,2048]{1,0:T(8,128)(2,1)} copy(bf16[64,2048]{1,0:T(8,128)(2,1)S(1)} %get-tuple-element.2) | data formatting | bytes 524288
  57.9 0.7 %copy.20 = bf16[256,512]{1,0:T(8,128)(2,1)} copy(bf16[256,512]{1,0:T(8,128)(2,1)S(1)} %get-tuple-element.3) | data formatting | bytes 524288

commit v5 on v4

--- a/solution.py
+++ b/solution.py
@@ -9,6 +9,7 @@
 
 HEAD_DIM = 128
 CHUNK = 64
+POOL = 24
 MESH = pl.DeviceIdType.MESH
 F32 = jnp.float32
 BF16 = jnp.bfloat16
@@ -70,22 +71,31 @@
         load.start()
 
     used = [0]
-
-    def remote(src, dst, device):
-        slot = used[0]
+    sent = []
+    idle = list(range(POOL))
+
+    def send_slot():
+        if idle:
+            return idle.pop(0)
+        copy, slot = sent.pop(0)
+        copy.wait_send()
+        return slot
+
+    def remote(src, dst, device, held=None):
+        recv, slot = used[0], send_slot() if held is None else held
         used[0] += 1
-        return pltpu.make_async_remote_copy(
-            src_ref=src, dst_ref=dst, send_sem=send_sem.at[slot], recv_sem=recv_sem.at[slot],
+        copy = pltpu.make_async_remote_copy(
+            src_ref=src, dst_ref=dst, send_sem=send_sem.at[slot], recv_sem=recv_sem.at[recv],
             device_id=device, device_id_type=MESH,
         )
-
-    sent = []
+        return copy, slot
+
+    def launch(made):
+        made[0].start()
+        sent.append(made)
+        return made[0]
+
     partner = (me, 2 * g + oc)
-
-    def launch(copy):
-        copy.start()
-        sent.append(copy)
-        return copy
 
     x = tok_ref[...].astype(F32)
     mean = jnp.mean(x, axis=-1, keepdims=True)
@@ -138,15 +148,16 @@
 
     dispatch = {}
 
-    far_base, back_base = used[0], used[0] + E
-    used[0] += 2 * E
-
-    def placed(src, dst, position, device, send, base):
+    far_base, back_base = used[0] - near, used[0] + E - near - 1
+    used[0] += E - near + E - 1
+
+    def placed(src, dst, position, device, slot, base):
         block = pl.ds(pl.multiple_of(position * cap, 16), cap)
-        return pltpu.make_async_remote_copy(
-            src_ref=src, dst_ref=dst(block), send_sem=send_sem.at[base + send],
+        copy = pltpu.make_async_remote_copy(
+            src_ref=src, dst_ref=dst(block), send_sem=send_sem.at[slot],
             recv_sem=recv_sem.at[base + position], device_id=device, device_id_type=MESH,
         )
+        return copy, slot
 
     def far_block(block):
         return feats.at[c, g, block]
@@ -158,20 +169,20 @@
         a, b = (to[i] for to in slots["to"])
         to = near + 2 * inner + (i - near) // 2 if swap else i
         src = outgoing.at[pl.ds((i - near) * cap, cap)]
-        launch(placed(src, far_block, to, (peer(a, b), t), i, far_base))
+        launch(placed(src, far_block, to, (peer(a, b), t), send_slot(), far_base))
 
     def far_arrived(i):
         src = outgoing.at[pl.ds((i - near) * cap, cap)]
-        placed(src, far_block, i, partner, i, far_base).wait_recv()
+        placed(src, far_block, i, partner, 0, far_base)[0].wait_recv()
 
     def send_back(i):
         a, b = (source[i] for source in slots["from"])
         to = near + inner + 2 * cross(i) if swap and i >= near else i
         src = fin.at[pl.ds(i * cap, cap)]
-        launch(placed(src, ret_block, to, (peer(a, b), t), i, back_base))
+        launch(placed(src, ret_block, to, (peer(a, b), t), send_slot(), back_base))
 
     def back_arrived(i):
-        placed(fin.at[pl.ds(i * cap, cap)], ret_block, i, partner, i, back_base).wait_recv()
+        placed(fin.at[pl.ds(i * cap, cap)], ret_block, i, partner, 0, back_base)[0].wait_recv()
 
     def send_near(i):
         dispatch[i] = launch(remote(
@@ -248,9 +259,14 @@
     pair = remote(ksend, krecv, (flip(me, 1), t))
     scan = E == 8
     if scan:
-        climb = remote(tsend, trecv, (lax.rem(me + 2, E), t))
-        hand = [remote(csend, crecv, (lax.rem(me + 2 + 2 * i, E), t)) for i in range(2)]
-    chain = remote(csend, crecv, (lax.rem(me + 2, E), t)) if Z > 1 and not scan else None
+        climb = remote(tsend, trecv, (lax.rem(me + 2, E), t), POOL)[0]
+        hand = [
+            remote(csend, crecv, (lax.rem(me + 2 + 2 * i, E), t), POOL + 1 + i)[0]
+            for i in range(2)
+        ]
+    chain = None
+    if Z > 1 and not scan:
+        chain = remote(csend, crecv, (lax.rem(me + 2, E), t), POOL)[0]
 
     def recurrence():
         for load in loads[:4]:
@@ -272,7 +288,7 @@
         launch(pair)
 
     def pair_end():
-        pair.wait_recv()
+        pair[0].wait_recv()
         s = krecv[:, 0:HEAD_DIM, :].astype(F32)
         d = krecv[:, HEAD_DIM:, :].astype(F32)
         bst[...] = jnp.where(odd, s, 0.0)
@@ -500,12 +516,13 @@
     }
     for step in plan:
         steps[step[0]](*step[1:])
+    assert used[0] <= recv_sem.shape[0]
     for i in range(1, E):
         back_arrived(i)
     exp_out[...] = lax.dot_general(
         wmat[...], ret[...], (((0,), (0,)), ((), ())), preferred_element_type=F32
     ).astype(BF16)
-    for copy in sent:
+    for copy, _ in sent:
         copy.wait_send()
     if scan:
         @pl.when(lax.rem(z, 2) == 0)
@@ -524,12 +541,12 @@
 
 
 STEPS = (
-    "f 4", "f 5", "f 6", "f 7", "p", "n 1", "h", "n 2", "l", "c 0", "a 4", "d 0",
+    "f 4", "f 5", "p", "n 1", "f 6", "f 7", "h", "n 2", "l", "c 0", "a 4", "d 0",
     "a 1", "c 1", "a 5", "b 4", "pair", "chain 0", "n 3", "d 1", "c 4", "b 5", "a 2", "a 6",
-    "d 4", "chain 1", "a 7",
-    "c 5", "d 5", "a 3", "e 0", "e 1", "c 2 3", "d 2", "d 3", "e 4", "chain 2", "b 6", "b 7",
-    "c 6 7", "d 6", "d 7", "e 5", "chains 3", "mc", "e 2", "e 6", "md", "e 7", "w", "e 3",
-    "me",
+    "d 4", "a 7",
+    "c 5", "chain 1", "d 5", "a 3", "e 0", "e 1", "c 2 3", "d 2", "d 3", "e 4", "chain 2", "b 6",
+    "b 7", "c 6 7", "d 6", "d 7", "e 5", "chains 3", "mc", "e 2", "e 6", "md", "e 7", "w",
+    "e 3", "me",
 )
 
 
@@ -555,7 +572,7 @@
     if E == 8:
         slots["to"] = (close + [6, 4, 7, 5], close + [4, 6, 5, 7])
         slots["from"] = (close + [6, 7, 4, 5], close + [4, 5, 6, 7])
-    copies = 3 * E + 4 + 8 * (G - 1 + G + 1 + G - 1) + G
+    copies = 2 * E - near - 1 + near - 1 + 8 + 4 * (2 * G - 1) + 9 * G
     vm = pl.BlockSpec(memory_space=pltpu.VMEM)
     anyspace = pl.BlockSpec(memory_space=pl.ANY)
     V = pltpu.VMEM
@@ -579,7 +596,7 @@
         V((tokens, width), BF16), V((2, G, R, D), BF16), V((G, R, D), BF16),
         V((max(G - 1, 1), R, D), BF16), V((max(G - 1, 1), R, D), BF16),
         pltpu.SemaphoreType.DMA((9,)),
-        pltpu.SemaphoreType.DMA((copies,)),
+        pltpu.SemaphoreType.DMA((POOL + 3,)),
         pltpu.SemaphoreType.DMA((copies,)),
     ]
     return pl.pallas_call(

time: 58.8 us -> 58 us (0.986)
  Pallas kernels: 56.6 us -> 55.8 us
    pallas_call x1, Pallas kernels: 56.6 us -> 55.8 us  [body(): pl.pallas_call(functools.partial(kernel, E, T, cap, near, slots, each, ma...]
where the time goes in v5:
time: 58 us; the launch traced here: 57.8 us
  Pallas kernels  55.8 us (96%)
  local copies, waits for them, and re-layouts  1.41 us (2%)
  between operations  0.65 us (1%)
    pallas_call x1, Pallas kernels, body(): pl.pallas_call(functools.partial(kernel, E, T, cap, near, slots, each, ma...  55.8 us
    unnamed x2, local copies, waits for them, and re-layouts  1.41 us

profile of v5, /device:TPU:9, one launch (start us, length us, event | category | flops | bytes accessed | tf_op | source)
XLA Modules:
  0.0 57.8 jit_solution(1902618165543950424)
XLA Ops:
  0.6 55.8 %shard_map.158 = (bf16[64,2048]{1,0:T(8,128)(2,1)S(1)}, bf16[256,512]{1,0:T(8,128)(2,1)S(1)}) custom-call(bf16[256,512]{1,0:T(8,128)(2,1)} %q_hbm.1, bf16[256,512]{1,0:T(8,128)(2,1)} %f_hbm.1, bf16[256,512]{1,0:T(8,128)(2,1)} %v_hbm.1, bf16[256,512]{1,0:T(8,128)(2,1)} %o_hbm.1, f32[1,512]{1,0:T(1,128)} %bitcast.12, f32[256,512]{1,0:T(8,128)} %extra_hbm.1, ...), custom_call_target="tpu_custom_call" | custom-call | tf_op jit(solution)/shard_map/pallas_call | solution.py:602
  56.4 0.7 %copy.19 = bf16[64,2048]{1,0:T(8,128)(2,1)} copy(bf16[64,2048]{1,0:T(8,128)(2,1)S(1)} %get-tuple-element.2) | data formatting | bytes 524288
  57.1 0.7 %copy.20 = bf16[256,512]{1,0:T(8,128)(2,1)} copy(bf16[256,512]{1,0:T(8,128)(2,1)S(1)} %get-tuple-element.3) | data formatting | bytes 524288

commit v6 on v5

--- a/solution.py
+++ b/solution.py
@@ -517,11 +517,15 @@
     for step in plan:
         steps[step[0]](*step[1:])
     assert used[0] <= recv_sem.shape[0]
-    for i in range(1, E):
-        back_arrived(i)
-    exp_out[...] = lax.dot_general(
-        wmat[...], ret[...], (((0,), (0,)), ((), ())), preferred_element_type=F32
-    ).astype(BF16)
+    total = 0.0
+    for lo, hi in ((0, near), (near, E)):
+        for i in range(max(lo, 1), hi):
+            back_arrived(i)
+        span = slice(lo * cap, hi * cap)
+        total += lax.dot_general(
+            wmat[span, :], ret[span, :], (((0,), (0,)), ((), ())), preferred_element_type=F32
+        )
+    exp_out[...] = total.astype(BF16)
     for copy, _ in sent:
         copy.wait_send()
     if scan:

time: 58 us -> 58.1 us (level)
  no operation moved by 1% of the time
where the time goes in v6:
time: 58.1 us; the launch traced here: 57.9 us
  Pallas kernels  55.9 us (96%)
  local copies, waits for them, and re-layouts  1.41 us (2%)
  between operations  0.65 us (1%)
    pallas_call x1, Pallas kernels, body(): pl.pallas_call(functools.partial(kernel, E, T, cap, near, slots, each, ma...  55.9 us
    unnamed x2, local copies, waits for them, and re-layouts  1.41 us

profile of v6, /device:TPU:9, one launch (start us, length us, event | category | flops | bytes accessed | tf_op | source)
XLA Modules:
  0.0 57.9 jit_solution(13855795248821521738)
XLA Ops:
  0.6 55.9 %shard_map.158 = (bf16[64,2048]{1,0:T(8,128)(2,1)S(1)}, bf16[256,512]{1,0:T(8,128)(2,1)S(1)}) custom-call(bf16[256,512]{1,0:T(8,128)(2,1)} %q_hbm.1, bf16[256,512]{1,0:T(8,128)(2,1)} %f_hbm.1, bf16[256,512]{1,0:T(8,128)(2,1)} %v_hbm.1, bf16[256,512]{1,0:T(8,128)(2,1)} %o_hbm.1, f32[1,512]{1,0:T(1,128)} %bitcast.12, f32[256,512]{1,0:T(8,128)} %extra_hbm.1, ...), custom_call_target="tpu_custom_call" | custom-call | tf_op jit(solution)/shard_map/pallas_call | solution.py:606
  56.5 0.7 %copy.19 = bf16[64,2048]{1,0:T(8,128)(2,1)} copy(bf16[64,2048]{1,0:T(8,128)(2,1)S(1)} %get-tuple-element.2) | data formatting | bytes 524288
  57.2 0.7 %copy.20 = bf16[256,512]{1,0:T(8,128)(2,1)} copy(bf16[256,512]{1,0:T(8,128)(2,1)S(1)} %get-tuple-element.3) | data formatting | bytes 524288
